TPU v7x, 32 devices: a whole 2x2x4 slice. The times are simulated.
32 devices in a mesh: sp: 8 (over z, x), tp: 4 (over y, core).
Axes of the slice: x: 2, y: 2, z: 4, core: 2. Of those that a mesh axis runs over, the one named last changes fastest.
Arguments:
- hidden_in: bfloat16 [2048, 2048], P('sp'), may hold values from -8 to 8
- w_convb: bfloat16 [2048, 1024], P('sp', 'tp'), may hold values from -0.125 to 0.125
- w_convc: bfloat16 [2048, 1024], P('sp', 'tp'), may hold values from -0.125 to 0.125
- w_convx: bfloat16 [2048, 1024], P('sp', 'tp'), may hold values from -0.125 to 0.125
- w_query: bfloat16 [2048, 1024], P('sp', 'tp'), may hold values from -1 to 1
- w_key: bfloat16 [2048, 1024], P('sp', 'tp'), may hold values from -1 to 1
- w_value: bfloat16 [2048, 1024], P('sp', 'tp'), may hold values from -0.125 to 0.125
- conv_taps: float32 [3, 1024], P(None, 'tp'), may hold values from -3.5 to 3.5
- gate_cache: float32 [2048, 16], P(None, 'tp'), as said below
- w_out_conv: bfloat16 [1024, 2048], P('tp'), may hold values from -0.125 to 0.125
- w_out_attn: bfloat16 [1024, 2048], P('tp'), may hold values from -0.125 to 0.125
Outputs:
- mixed: bfloat16 [2048, 2048], P(('sp', 'tp'))
Inputs may be any that keep to these rules, and one draw needn't show every extreme that they name: `gate_cache`: down each column, read from row 256 to the last row and then from row 0 on, the values never rise.
All inputs are finite; a program needn't handle non-finite values.
Results may differ from a plain program's by a relative error of at most 0.018.
Values may be sent and summed in bfloat16 or wider, within the bound.
A program may use at most 128 MiB of HBM per device.

v0:
```python
import jax
import jax.numpy as jnp
from jax import lax
from jax.sharding import PartitionSpec as P

neg_large = -1e30


def passed_along(value, axis, steps):
    count = lax.axis_size(axis)
    pairs = [(source, (source + steps) % count) for source in range(count)]
    return lax.ppermute(value, axis, pairs)


def shortened(shard):

    def short(part):
        return part.astype(jnp.bfloat16) if part.dtype == jnp.float32 else part

    return jax.tree.map(short, shard)


def project(weight_rows, hidden_in):
    return jnp.dot(hidden_in, weight_rows, preferred_element_type=jnp.float32)


def absorb(attn_state, query_heads, gate_rows, key_heads, value_heads, gate_cols, allowed):
    running_max, row_total, weighted = attn_state
    score_scale = query_heads.shape[2] ** (-0.5)
    scores = (
        jnp.einsum("qhd,khd->hqk", query_heads, key_heads, preferred_element_type=jnp.float32)
        * score_scale
    )
    scores = scores + gate_rows.T[:, :, None] - gate_cols.T[:, None, :]
    if allowed is not None:
        scores = jnp.where(allowed[None], scores, neg_large)
    new_max = jnp.maximum(running_max, jnp.max(scores, axis=2))
    weights = jnp.exp(scores - new_max[:, :, None])
    factor = jnp.exp(running_max - new_max)
    row_total = row_total * factor + jnp.sum(weights, axis=2)
    weighted = weighted * factor[:, :, None] + jnp.einsum(
        "hqk,khd->hqd",
        weights.astype(jnp.bfloat16),
        value_heads,
        preferred_element_type=jnp.float32,
    )
    return (new_max, row_total, weighted)


def shards(
    hidden_in,
    w_convb,
    w_convc,
    w_convx,
    w_query,
    w_key,
    w_value,
    conv_taps,
    gate_cache,
    w_out_conv,
    w_out_attn,
):
    tok_rows = hidden_in.shape[0]
    head_count = gate_cache.shape[1]
    attn_width = w_query.shape[1]
    head_depth = attn_width // head_count
    axis_length = lax.axis_size("sp")
    group_span = axis_length // 4
    seq_index = lax.axis_index("sp")
    position = (seq_index - group_span // 2) % group_span
    pieces = (
        lax.all_gather(w_convb, "sp", axis=0, tiled=True),
        lax.all_gather(w_convc, "sp", axis=0, tiled=True),
        lax.all_gather(w_convx, "sp", axis=0, tiled=True),
        lax.all_gather(w_query, "sp", axis=0, tiled=True),
        lax.all_gather(w_key, "sp", axis=0, tiled=True),
        lax.all_gather(w_value, "sp", axis=0, tiled=True),
    )
    projected = tuple((project(weight_rows, hidden_in) for weight_rows in pieces))
    gate_b, gate_c, conv_values, query, keys, values = [
        partial_total.astype(jnp.bfloat16) for partial_total in projected
    ]
    conv_input = (gate_c.astype(jnp.float32) * conv_values.astype(jnp.float32)).astype(jnp.bfloat16)
    last_rows = conv_input[tok_rows - 2 :]
    query_heads = query.reshape(tok_rows, head_count, head_depth)
    key_heads = keys.reshape(tok_rows, head_count, head_depth)
    value_heads = values.reshape(tok_rows, head_count, head_depth)
    gate_rows = lax.dynamic_slice_in_dim(gate_cache, seq_index * tok_rows, tok_rows, 0)

    def gates_back(distance):
        source = (seq_index - distance + axis_length) % axis_length
        return lax.dynamic_slice_in_dim(gate_cache, source * tok_rows, tok_rows, 0)

    row_ids = jnp.arange(tok_rows, dtype=jnp.int32)
    allowed = row_ids[None, :] <= row_ids[:, None]
    initial = (
        jnp.full((head_count, tok_rows), neg_large, jnp.float32),
        jnp.zeros((head_count, tok_rows), jnp.float32),
        jnp.zeros((head_count, tok_rows, head_depth), jnp.float32),
    )
    attn_state = absorb(initial, query_heads, gate_rows, key_heads, value_heads, gate_rows, allowed)
    edge_rows = passed_along(last_rows, "sp", 1)
    payload = (key_heads, value_heads)
    arrived = jax.tree.map(
        lambda part, own: part.astype(own.dtype), passed_along(shortened(payload), "sp", 1), payload
    )
    travel = (arrived[0], arrived[1])
    first_gates = gates_back(1)
    attn_state = lax.cond(
        position >= 1,
        lambda current: absorb(
            current, query_heads, gate_rows, travel[0], travel[1], first_gates, None
        ),
        lambda current: current,
        attn_state,
    )

    def relay_turn(turn_index, carried):
        present_memory, moving = carried
        moving = passed_along((moving[0], moving[1]), "sp", 1)
        source_gates = gates_back(turn_index)
        present_memory = lax.cond(
            turn_index <= position,
            lambda present: absorb(
                present, query_heads, gate_rows, moving[0], moving[1], source_gates, None
            ),
            lambda present: present,
            present_memory,
        )
        return (present_memory, moving)

    attn_state, travel = lax.fori_loop(2, group_span, relay_turn, (attn_state, travel))
    edge_rows = jnp.where(position > 0, edge_rows, jnp.zeros_like(edge_rows))
    padded = lax.optimization_barrier(jnp.concatenate([edge_rows, conv_input], axis=0)).astype(
        jnp.float32
    )
    mixed_conv = (
        conv_taps[0] * padded[:tok_rows]
        + conv_taps[1] * padded[1 : tok_rows + 1]
        + conv_taps[2] * padded[2:]
    )
    conv_out = (gate_b.astype(jnp.float32) * mixed_conv).astype(jnp.bfloat16)
    running_max, row_total, weighted = attn_state
    attn_out = (
        (weighted / row_total[:, :, None])
        .transpose(1, 0, 2)
        .reshape(tok_rows, attn_width)
        .astype(jnp.bfloat16)
    )
    return lax.psum_scatter(
        (
            jnp.dot(conv_out, w_out_conv, preferred_element_type=jnp.float32)
            + jnp.dot(attn_out, w_out_attn, preferred_element_type=jnp.float32)
        ).astype(jnp.bfloat16),
        "tp",
        scatter_dimension=0,
        tiled=True,
    )


def solution(mesh):
    return jax.shard_map(
        shards,
        mesh=mesh,
        in_specs=(
            P("sp", None),
            P("sp", "tp"),
            P("sp", "tp"),
            P("sp", "tp"),
            P("sp", "tp"),
            P("sp", "tp"),
            P("sp", "tp"),
            P(None, "tp"),
            P(None, "tp"),
            P("tp", None),
            P("tp", None),
        ),
        out_specs=P(("sp", "tp"), None),
        check_vma=False,
    )
```

profile of v0, /device:TPU:0, one launch (start us, length us, event | category | flops | bytes accessed | tf_op | source)
XLA Modules:
  0.0 297.6 jit_solution(8631214594940735068)
XLA Ops:
  6.5 0.0 copy-start
  6.5 0.0 all-gather.15.cloned.1.call-start
  6.5 0.7 all-gather.15.cloned.1.call-update
  7.3 0.0 all-gather.17.cloned.1.call-start
  7.3 0.7 all-gather.17.cloned.1.call-update
  8.0 0.0 all-gather.9.cloned.1.call-start
  8.1 0.7 all-gather.9.cloned.1.call-update
  8.7 0.0 all-gather.11.cloned.1.call-start
  8.8 0.5 all-gather.11.cloned.1.call-update
  9.3 0.0 all-gather.13.cloned.1.call-start
  9.4 0.5 all-gather.13.cloned.1.call-update
  9.9 0.0 all-gather.7.cloned.1.call-start
  10.0 0.5 all-gather.7.cloned.1.call-update
  10.5 0.0 reduce-scatter.2.cloned.1.call-start
  10.6 0.7 fusion.54
  11.3 0.7 constant_dynamic-slice_fusion
  12.0 1.4 fusion.31
  13.3 39.2 %all-gather.15.cloned.1.call-done = bf16[2048,256]{1,0:T(8,128)(2,1)} async-done(((bf16[256,256]{1,0:T(8,128)(2,1)}), bf16[2048,256]{1,0:T(8,128)(2,1)}) %all-gather.15.cloned.1.call-update) | async-done | bytes 1048592 | tf_op jit(solution)/shard_map/all_gather | solution.py:76
  52.5 0.0 copy-done
  52.5 2.4 convolution_convert_fusion.1
  54.9 0.6 collective-permute-start.1
  55.5 38.2 %all-gather.17.cloned.1.call-done = bf16[2048,256]{1,0:T(8,128)(2,1)} async-done(((bf16[256,256]{1,0:T(8,128)(2,1)}), bf16[2048,256]{1,0:T(8,128)(2,1)}) %all-gather.17.cloned.1.call-update) | async-done | bytes 1048592 | tf_op jit(solution)/shard_map/all_gather | solution.py:77
  93.6 2.4 convolution_convert_fusion
  96.1 0.6 collective-permute-start.2
  96.6 38.1 %all-gather.9.cloned.1.call-done = bf16[2048,256]{1,0:T(8,128)(2,1)} async-done(((bf16[256,256]{1,0:T(8,128)(2,1)}), bf16[2048,256]{1,0:T(8,128)(2,1)}) %all-gather.9.cloned.1.call-update) | async-done | bytes 1048592 | tf_op jit(solution)/shard_map/all_gather | solution.py:73
  134.8 1.7 fusion.13
  136.5 39.3 %all-gather.11.cloned.1.call-done = bf16[2048,256]{1,0:T(8,128)(2,1)} async-done(((bf16[256,256]{1,0:T(8,128)(2,1)}), bf16[2048,256]{1,0:T(8,128)(2,1)}) %all-gather.11.cloned.1.call-update) | async-done | bytes 1048592 | tf_op jit(solution)/shard_map/all_gather | solution.py:74
  175.8 1.7 fusion.12
  177.5 0.6 collective-permute-start
  178.1 38.7 %all-gather.13.cloned.1.call-done = bf16[2048,256]{1,0:T(8,128)(2,1)} async-done(((bf16[256,256]{1,0:T(8,128)(2,1)}), bf16[2048,256]{1,0:T(8,128)(2,1)}) %all-gather.13.cloned.1.call-update) | async-done | bytes 1048592 | tf_op jit(solution)/shard_map/all_gather | solution.py:75
  216.8 1.7 convolution_convert_fusion.2
  218.5 1.3 fusion.32
  219.9 0.2 fusion.19
  220.1 1.2 convolution_add_fusion.2
  221.3 0.0 collective-permute-done
  221.3 0.7 convert_element_type.68
  222.1 35.7 %all-gather.7.cloned.1.call-done = bf16[2048,256]{1,0:T(8,128)(2,1)} async-done(((bf16[256,256]{1,0:T(8,128)(2,1)}), bf16[2048,256]{1,0:T(8,128)(2,1)}) %all-gather.7.cloned.1.call-update) | async-done | bytes 1048592 | tf_op jit(solution)/shard_map/all_gather | solution.py:72
  257.8 3.1 %fusion.17 = f32[256,2048]{1,0:T(8,128)S(1)} fusion(bf16[256,2048]{1,0:T(8,128)(2,1)} %param.22, bf16[256,2048]{1,0:T(8,128)(2,1)S(1)} %copy-done, bf16[2048,256]{1,0:T(8,128)(2,1)} %all-gather.7.cloned.1.call-done, f32[258,256]{1,0:T(8,128)} %convert_element_type.68, f32[256]{0:T(256)} %bitcast.42, f32[256]{0:T(256)} %bitcast.43, f32[256]{0:T(256)S(1)} %bitcast.41), kind=kOutput, calls=%fused_computation.31 | convolution fusion | flops 537460736 | bytes 6032384 | tf_op jit(solution)/shard_map/dot_general | solution.py:152
  260.9 0.0 collective-permute-done.1
  260.9 0.0 collective-permute-done.2
  260.9 3.4 %conditional.1 = ((f32[4,256]{1,0:T(4,128)S(1)}, f32[4,256,64]{1,2,0:T(8,128)S(1)})) conditional(s32[]{:T(128)} %convert_element_type.70, (f32[4,256]{1,0:T(4,128)S(1)}, f32[4,256,64]{1,2,0:T(8,128)S(1)}) %tuple.26, (bf16[256,4,64]{0,2,1:T(8,128)(2,1)S(1)}, bf16[256,4,64]{0,2,1:T(8,128)(2,1)}, f32[256,4]{0,1:T(4,128)S(1)}, s32[]{:T(128)}, ...), branch_computations={%region_2.3_spmd, %region_3.6_spmd.clone} | conditional | flops 69339152 | bytes 4137155 | solution.py:109
  260.9 0.7 dynamic-slice_bitcast_fusion
  261.6 1.3 fusion.30
  262.9 0.2 fusion.3
  263.1 1.2 convolution_add_fusion
  264.4 2.7 fusion.6
  267.0 0.0 reduce-scatter.2.cloned.1.call-update
  267.1 23.7 %reduce-scatter.2.cloned.1.call-done = bf16[64,2048]{1,0:T(8,128)(2,1)} async-done(((bf16[256,2048]{1,0:T(8,128)(2,1)}), bf16[64,2048]{1,0:T(8,128)(2,1)}) %reduce-scatter.2.cloned.1.call-update) | async-done | bytes 262160 | tf_op jit(solution)/shard_map/reduce_scatter | solution.py:150
  (9 shorter events, 0.1 us)
Async XLA Ops:
  6.5 46.0 %copy-start = (bf16[256,2048]{1,0:T(8,128)(2,1)S(1)}, bf16[256,2048]{1,0:T(8,128)(2,1)}, u32[]{:S(2)}) copy-start(bf16[256,2048]{1,0:T(8,128)(2,1)} %param.13) | copy-start | bytes 3145732
  6.5 46.0 %all-gather.15.cloned.1.call-start = ((), (), s32[]{:S(2)}) async-start(), calls=%async_computation.5 | async-start | bytes 1179648 | tf_op jit(solution)/shard_map/all_gather | solution.py:76
  7.3 86.4 %all-gather.17.cloned.1.call-start = ((), (), s32[]{:S(2)}) async-start(), calls=%async_computation.6 | async-start | bytes 1179648 | tf_op jit(solution)/shard_map/all_gather | solution.py:77
  8.0 126.8 %all-gather.9.cloned.1.call-start = ((), (), s32[]{:S(2)}) async-start(), calls=%async_computation.2 | async-start | bytes 1179648 | tf_op jit(solution)/shard_map/all_gather | solution.py:73
  8.7 167.0 %all-gather.11.cloned.1.call-start = ((), (), s32[]{:S(2)}) async-start(), calls=%async_computation.3 | async-start | bytes 1179648 | tf_op jit(solution)/shard_map/all_gather | solution.py:74
  9.3 207.5 %all-gather.13.cloned.1.call-start = ((), (), s32[]{:S(2)}) async-start(), calls=%async_computation.4 | async-start | bytes 1179648 | tf_op jit(solution)/shard_map/all_gather | solution.py:75
  9.9 247.9 %all-gather.7.cloned.1.call-start = ((), (), s32[]{:S(2)}) async-start(), calls=%async_computation.1 | async-start | bytes 1179648 | tf_op jit(solution)/shard_map/all_gather | solution.py:72
  10.5 280.3 %reduce-scatter.2.cloned.1.call-start = ((), (), s32[]{:S(2)}) async-start(), calls=%async_computation.7 | async-start | bytes 1310720 | tf_op jit(solution)/shard_map/reduce_scatter | solution.py:150
  54.9 206.0 %collective-permute-start.1 = (bf16[256,4,64]{0,2,1:T(8,128)(2,1)}, bf16[256,4,64]{0,2,1:T(8,128)(2,1)}, u32[]{:S(2)}, u32[]{:S(2)}) collective-permute-start(bf16[256,4,64]{0,2,1:T(8,128)(2,1)} %bitcast.6), channel_id=1, source_target_pairs={{0,4},{4,8},{8,12},{12,16},{16,20},{20,24},{24,28},{28,0},{1,5},{5... | collective-permute-start | bytes 393224 | tf_op jit(solution)/shard_map/ppermute | solution.py:12
  96.1 164.8 %collective-permute-start.2 = (bf16[256,4,64]{0,2,1:T(8,128)(2,1)}, bf16[256,4,64]{0,2,1:T(8,128)(2,1)}, u32[]{:S(2)}, u32[]{:S(2)}) collective-permute-start(bf16[256,4,64]{0,2,1:T(8,128)(2,1)} %bitcast.8), channel_id=1, source_target_pairs={{0,4},{4,8},{8,12},{12,16},{16,20},{20,24},{24,28},{28,0},{1,5},{5... | collective-permute-start | bytes 393224 | tf_op jit(solution)/shard_map/ppermute | solution.py:12
  177.5 43.8 %collective-permute-start = (bf16[2,256]{1,0:T(2,128)(2,1)S(1)}, bf16[2,256]{1,0:T(2,128)(2,1)S(1)}, u32[]{:S(2)}, u32[]{:S(2)}) collective-permute-start(bf16[2,256]{1,0:T(2,128)(2,1)S(1)} %slice.28), channel_id=1, source_target_pairs={{0,4},{4,8},{8,12},{12,16},{16,20},{20,24},{24,28},{28,0},{1,5},{5... | collective-permute-start | bytes 3080 | tf_op jit(solution)/shard_map/ppermute | solution.py:12
Sparse Core Ops, SparseCore 0:
  9.5 42.9 all-gather.14
  54.6 38.9 all-gather.16
  95.8 38.9 all-gather.8
  136.8 38.9 all-gather.10
  177.8 38.9 all-gather.12
  218.8 38.9 all-gather.6
  267.2 23.5 reduce-scatter.1
where the time goes:
time: 298 us
  waiting for transfers between devices  257 us (86%)
  matrix products  20.7 us (7%)
  between operations  13.6 us (5%)
  local copies, waits for them, and re-layouts  3.45 us (1%)
    all_gather x1, waiting for transfers between devices, shards(): lax.all_gather(w_convx, 'sp', axis=0, tiled=True)  39.3 us
    all_gather x1, waiting for transfers between devices, shards(): lax.all_gather(w_key, 'sp', axis=0, tiled=True)  39.2 us
    all_gather x1, waiting for transfers between devices, shards(): lax.all_gather(w_query, 'sp', axis=0, tiled=True)  38.7 us
    all_gather x1, waiting for transfers between devices, shards(): lax.all_gather(w_value, 'sp', axis=0, tiled=True)  38.2 us
    all_gather x1, waiting for transfers between devices, shards(): lax.all_gather(w_convc, 'sp', axis=0, tiled=True)  38.1 us
    all_gather x1, waiting for transfers between devices, shards(): lax.all_gather(w_convb, 'sp', axis=0, tiled=True)  35.7 us
    reduce_scatter x1, waiting for transfers between devices, shards(): lax.psum_scatter((jnp.dot(conv_out, w_out_conv, preferred_element_type=jn...  23.7 us
    dot_general x5, matrix products, project(): return jnp.dot(hidden_in, weight_rows, preferred_element_type=jnp.float32)  9.89 us
  transfers between devices with their start and end apart: 10, of which 7 were waited for; matrix products, arithmetic and copies ran while one was open for 6% of the time, Pallas kernels for 0%

commit v1 on v0

--- a/solution.py
+++ b/solution.py
@@ -1,6 +1,10 @@
+import functools
+
 import jax
 import jax.numpy as jnp
 from jax import lax
+from jax.experimental import pallas as pl
+from jax.experimental.pallas import tpu as pltpu
 from jax.sharding import PartitionSpec as P
 
 neg_large = -1e30
@@ -158,9 +162,546 @@
     )
 
 
+MESH = pl.DeviceIdType.MESH
+N_CHUNKS = 4
+
+
+def fused_kernel(
+    small_ref,
+    hidden_ref,
+    wq_ref,
+    wk_ref,
+    wv_ref,
+    wc_ref,
+    wx_ref,
+    wb_ref,
+    woa_ref,
+    woc_ref,
+    out_ref,
+    hbuf,
+    wbuf,
+    small,
+    proj,
+    woa,
+    woc,
+    acts,
+    act_in,
+    pbuf,
+    rx_core,
+    y_send,
+    y_recv,
+    s_small,
+    r_small,
+    s_w,
+    r_w,
+    s_wx,
+    s_wc,
+    s_hx,
+    s_hz,
+    s_hy,
+    r_h,
+    s_act,
+    r_act,
+    s_core,
+    r_core,
+    s_y,
+    r_y,
+    l_wo,
+):
+    sp = lax.axis_index("sp")
+    tp = lax.axis_index("tp")
+    z, x = sp // 2, sp % 2
+    y, c = tp // 2, tp % 2
+    rows = hidden_ref.shape[0]
+    half_rows = rows // 2
+    half_h = z % 2
+    owner_core = z // 2
+
+    def at(zz, xx, yy, cc):
+        return {"sp": zz * 2 + xx, "tp": yy * 2 + cc}
+
+    def remote(src, dst, ss, rs, dev):
+        return pltpu.make_async_remote_copy(
+            src_ref=src, dst_ref=dst, send_sem=ss, recv_sem=rs, device_id=dev, device_id_type=MESH
+        )
+
+    core_mate = at(z, x, y, 1 - c)
+    x_mate = at(z, 1 - x, y, c)
+    y_mate = at(z, x, 1 - y, c)
+
+    barrier = pltpu.get_barrier_semaphore()
+
+    @pl.loop(0, 8)
+    def _(s):
+        for cc in range(2):
+            pl.semaphore_signal(
+                barrier, inc=1, device_id={"sp": s, "tp": y * 2 + cc}, device_id_type=MESH
+            )
+
+    pl.semaphore_signal(barrier, inc=1, device_id=y_mate, device_id_type=MESH)
+    pl.semaphore_wait(barrier, 17)
+
+    root_z = (2 * c + x, (2 * c + x + 1) % 4)
+    root_x = (1, 0)
+    block_of = (root_z[0] * 2 + 1, root_z[1] * 2)
+    seq_mine = ((sp + 7) % 8) // 2
+    x_mine, c_mine = seq_mine % 2, seq_mine // 2
+    my_rows = pl.ds(pl.multiple_of(y * half_rows, half_rows), half_rows)
+    other_rows = pl.ds(pl.multiple_of((1 - y) * half_rows, half_rows), half_rows)
+
+    def fan_out(i, src, go):
+        for step in range(1, 4):
+            zz = (z + step) % 4
+            copy = remote(src, hbuf.at[i, my_rows], s_hz.at[i, step - 1], r_h.at[i, 0], at(zz, x, y, c))
+            go(copy)
+
+    def start(copy):
+        copy.start()
+
+    for i in range(2):
+        is_root = z == root_z[i]
+
+        @pl.when(is_root & (x == root_x[i]))
+        def _():
+            fan_out(i, hidden_ref.at[my_rows], start)
+            pltpu.make_async_copy(
+                hidden_ref.at[my_rows], hbuf.at[i, my_rows], r_h.at[i, 0]
+            ).start()
+            pltpu.make_async_copy(
+                hidden_ref.at[other_rows], hbuf.at[i, other_rows], r_h.at[i, 1]
+            ).start()
+
+    def inject_copy():
+        slot = 1 - x
+        return remote(
+            hidden_ref.at[my_rows], hbuf.at[slot, my_rows], s_hx, r_h.at[slot, 0], x_mate
+        )
+
+    injects = (c == c_mine) & (x_mine != x)
+
+    @pl.when(injects)
+    def _():
+        inject_copy().start()
+
+    sources = (wq_ref, wk_ref, wv_ref, wc_ref, wx_ref, wb_ref)
+
+    def tile(j, s, cc):
+        return wbuf.at[
+            j,
+            pl.ds(pl.multiple_of(s * rows, rows), rows),
+            pl.ds(pl.multiple_of(cc * 128, 128), 128),
+        ]
+
+    def own_tile(j, cc, h):
+        src = sources[2 * j + cc].at[:, pl.ds(h * 128, 128)]
+        zt = 2 * c + h
+        return zt, src, remote(
+            src, tile(j, sp, cc), s_w.at[j, cc, h], r_w.at[j, sp, cc], at(zt, x, y, cc)
+        )
+
+    for j in range(3):
+        for cc in range(2):
+            for h in range(2):
+                zt, src, copy = own_tile(j, cc, h)
+                keep = (zt == z) & (c == cc)
+
+                @pl.when(keep)
+                def _():
+                    pltpu.make_async_copy(src, tile(j, sp, cc), r_w.at[j, sp, cc]).start()
+
+                @pl.when(jnp.logical_not(keep))
+                def _():
+                    copy.start()
+
+    small_copy = remote(small_ref, small, s_small, r_small, core_mate)
+
+    @pl.when(c == owner_core)
+    def _():
+        small_copy.start()
+        pltpu.make_async_copy(small_ref, small, r_small).start()
+
+    wo_copies = (
+        pltpu.make_async_copy(woa_ref, woa, l_wo.at[0]),
+        pltpu.make_async_copy(woc_ref, woc, l_wo.at[1]),
+    )
+    for copy in wo_copies:
+        copy.start()
+
+    def hid_y(i):
+        return remote(
+            hbuf.at[i, my_rows], hbuf.at[i, my_rows], s_hy.at[i], r_h.at[i, 1], y_mate
+        )
+
+    def hid_wait(i, k, part):
+        remote(hbuf.at[i, part], hbuf.at[i, part], s_hy.at[i], r_h.at[i, k], y_mate).wait_recv()
+
+    def has_local(i):
+        return (z == root_z[i]) & (x == root_x[i])
+
+    for i in range(2):
+
+        @pl.when((z == root_z[i]) & (x != root_x[i]))
+        def _():
+            hid_wait(i, 0, my_rows)
+            fan_out(i, hbuf.at[i, my_rows], start)
+            hid_y(i).start()
+
+    def fwd_x(j, zz):
+        t = tile(j, zz * 2 + x, c)
+        return remote(t, t, s_wx.at[j, zz], r_w.at[j, zz * 2 + x, c], x_mate)
+
+    def fwd_core(j, s):
+        t = tile(j, s, c)
+        return remote(t, t, s_wc.at[j, s], r_w.at[j, s, c], core_mate)
+
+    def tile_wait(j, s, cc):
+        t = tile(j, s, cc)
+        remote(t, t, s_wc.at[j, s], r_w.at[j, s, cc], core_mate).wait_recv()
+
+    def line_forward(j):
+        @pl.loop(0, 4)
+        def _(k):
+            zz = (z + k) % 4
+            tile_wait(j, zz * 2 + x, c)
+            fwd_x(j, zz).start()
+            fwd_core(j, zz * 2 + x).start()
+
+    def cross_forward(j):
+        @pl.loop(0, 4)
+        def _(k):
+            zz = (z + k) % 4
+            tile_wait(j, zz * 2 + 1 - x, c)
+            fwd_core(j, zz * 2 + 1 - x).start()
+
+    def mate_wait(j):
+        @pl.loop(0, 8)
+        def _(s):
+            tile_wait(j, s, 1 - c)
+
+    def project_pair(j):
+        @pl.loop(0, 2)
+        def _(i):
+            proj[j, i] = jnp.dot(
+                hbuf[i], wbuf[j], preferred_element_type=jnp.float32
+            ).astype(jnp.bfloat16)
+
+    line_forward(0)
+    for i in range(2):
+
+        @pl.when(z != root_z[i])
+        def _():
+            hid_wait(i, 0, my_rows)
+            hid_y(i).start()
+
+        @pl.when(has_local(i))
+        def _():
+            hid_wait(i, 0, my_rows)
+
+    cross_forward(0)
+    line_forward(1)
+    cross_forward(1)
+    for i in range(2):
+        hid_wait(i, 1, other_rows)
+    mate_wait(0)
+    project_pair(0)
+    mate_wait(1)
+    project_pair(1)
+    line_forward(2)
+    cross_forward(2)
+
+    pltpu.make_async_copy(small_ref, small, r_small).wait()
+
+    depth = 64
+    lane_head = lax.broadcasted_iota(jnp.int32, (rows, 128), 1) // depth
+    gates = [
+        small[:, pl.ds(pl.multiple_of(block_of[i] * rows, rows), rows)] for i in range(2)
+    ]
+    gates_t = [g.T for g in gates]
+    causal = lax.broadcasted_iota(jnp.int32, (rows, rows), 0) >= lax.broadcasted_iota(
+        jnp.int32, (rows, rows), 1
+    )
+    first = half_h == 0
+    for i in range(2):
+        q = proj[0, i, :, :128]
+        merged = None
+        for hh in range(2):
+            col = jnp.where(first, gates_t[i][:, hh : hh + 1], gates_t[i][:, 2 + hh : 3 + hh])
+            scores = []
+            for k in range(i + 1):
+                keys = proj[0, k, :, 128:]
+                keys = jnp.where(lane_head == hh, keys, jnp.zeros_like(keys))
+                row = jnp.where(first, gates[k][hh : hh + 1], gates[k][2 + hh : 3 + hh])
+                s = (
+                    lax.dot_general(
+                        q, keys, (((1,), (1,)), ((), ())), preferred_element_type=jnp.float32
+                    )
+                    * depth ** (-0.5)
+                    + col
+                    - row
+                )
+                if k == i:
+                    s = jnp.where(causal, s, neg_large)
+                scores.append(s)
+            top = jnp.max(scores[0], axis=1, keepdims=True)
+            for s in scores[1:]:
+                top = jnp.maximum(top, jnp.max(s, axis=1, keepdims=True))
+            total, weighted = None, None
+            for k, s in enumerate(scores):
+                w = jnp.exp(s - top)
+                t = jnp.sum(w, axis=1, keepdims=True)
+                a = jnp.dot(
+                    w.astype(jnp.bfloat16), proj[1, k, :, :128], preferred_element_type=jnp.float32
+                )
+                total = t if total is None else total + t
+                weighted = a if weighted is None else weighted + a
+            done = weighted / total
+            merged = done if merged is None else jnp.where(lane_head == 0, merged, done)
+        acts[0, i] = merged.astype(jnp.bfloat16)
+
+    lanes_h = pl.ds(pl.multiple_of(half_h * 128, 128), 128)
+
+    def act_copy(kind, i):
+        return remote(
+            acts.at[kind, i],
+            act_in.at[kind, :, lanes_h],
+            s_act.at[kind, i],
+            r_act.at[kind, half_h],
+            at(root_z[i], root_x[i], y, owner_core),
+        )
+
+    def act_stays(i):
+        return has_local(i) & (c == owner_core)
+
+    def send_acts(kind):
+        for i in range(2):
+
+            @pl.when(act_stays(i))
+            def _():
+                pltpu.make_async_copy(
+                    acts.at[kind, i], act_in.at[kind, :, lanes_h], r_act.at[kind, half_h]
+                ).start()
+
+            @pl.when(jnp.logical_not(act_stays(i)))
+            def _():
+                act_copy(kind, i).start()
+
+    def wait_acts(kind):
+        for h in range(2):
+            remote(
+                acts.at[kind, 0],
+                act_in.at[kind, :, pl.ds(h * 128, 128)],
+                s_act.at[kind, 0],
+                r_act.at[kind, h],
+                core_mate,
+            ).wait_recv()
+
+    send_acts(0)
+
+    mate_wait(2)
+    project_pair(2)
+    row_id = lax.broadcasted_iota(jnp.int32, (2 * rows, 128), 0)
+    gate_c = jnp.concatenate([proj[1, 0, :, 128:], proj[1, 1, :, 128:]], axis=0)
+    conv_v = jnp.concatenate([proj[2, 0, :, :128], proj[2, 1, :, :128]], axis=0)
+    gate_b = jnp.concatenate([proj[2, 0, :, 128:], proj[2, 1, :, 128:]], axis=0)
+    conv_in = (
+        (gate_c.astype(jnp.float32) * conv_v.astype(jnp.float32))
+        .astype(jnp.bfloat16)
+        .astype(jnp.float32)
+    )
+    taps = [jnp.where(first, small[4 + k : 5 + k, :128], small[4 + k : 5 + k, 128:256]) for k in range(3)]
+    mixed = taps[2] * conv_in
+    for back in (1, 2):
+        moved = jnp.where(row_id >= back, pltpu.roll(conv_in, back, 0), 0.0)
+        mixed = mixed + taps[2 - back] * moved
+    conv_out = (gate_b.astype(jnp.float32) * mixed).astype(jnp.bfloat16)
+    acts[1, 0] = conv_out[:rows]
+    acts[1, 1] = conv_out[rows:]
+    send_acts(1)
+
+    for copy in wo_copies:
+        copy.wait()
+    wait_acts(0)
+    wait_acts(1)
+
+    part_rows = pbuf.shape[2]
+    width = pbuf.shape[3] // N_CHUNKS
+
+    def cols(n):
+        return pl.ds(n * width, width)
+
+    def core_copy(n):
+        return remote(
+            pbuf.at[:, 1 - c, :, cols(n)],
+            rx_core.at[:, :, cols(n)],
+            s_core.at[n],
+            r_core.at[n],
+            core_mate,
+        )
+
+    def y_copy(n):
+        return remote(y_send.at[:, cols(n)], y_recv.at[:, cols(n)], s_y.at[n], r_y.at[n], y_mate)
+
+    def out_chunk(n):
+        part = jnp.dot(
+            act_in[0], woa[:, cols(n)], preferred_element_type=jnp.float32
+        ) + jnp.dot(act_in[1], woc[:, cols(n)], preferred_element_type=jnp.float32)
+        part = part.astype(jnp.bfloat16)
+        for yy in range(2):
+            for cc in range(2):
+                first_row = (yy * 2 + cc) * part_rows
+                pbuf[yy, cc, :, cols(n)] = part[first_row : first_row + part_rows]
+        core_copy(n).start()
+
+    def pass_chunk(n):
+        core_copy(n).wait_recv()
+        y_send[:, cols(n)] = (
+            pbuf[1 - y, c, :, cols(n)].astype(jnp.float32)
+            + rx_core[1 - y, :, cols(n)].astype(jnp.float32)
+        ).astype(jnp.bfloat16)
+        y_copy(n).start()
+
+    for n in range(N_CHUNKS):
+        out_chunk(n)
+        if n >= 1:
+            pass_chunk(n - 1)
+    pass_chunk(N_CHUNKS - 1)
+    for n in range(N_CHUNKS):
+        y_copy(n).wait_recv()
+        out_ref[:, cols(n)] = (
+            pbuf[y, c, :, cols(n)].astype(jnp.float32)
+            + rx_core[y, :, cols(n)].astype(jnp.float32)
+            + y_recv[:, cols(n)].astype(jnp.float32)
+        ).astype(jnp.bfloat16)
+
+    for n in range(N_CHUNKS):
+        core_copy(n).wait_send()
+        y_copy(n).wait_send()
+    for kind in range(2):
+        for i in range(2):
+
+            @pl.when(jnp.logical_not(act_stays(i)))
+            def _():
+                act_copy(kind, i).wait_send()
+
+    @pl.when(c == owner_core)
+    def _():
+        small_copy.wait_send()
+
+    @pl.when(injects)
+    def _():
+        inject_copy().wait_send()
+
+    for i in range(2):
+
+        @pl.when(z == root_z[i])
+        def _():
+            fan_out(i, hbuf.at[i, my_rows], lambda copy: copy.wait_send())
+
+        @pl.when(jnp.logical_not(has_local(i)))
+        def _():
+            hid_y(i).wait_send()
+
+    for j in range(3):
+        for cc in range(2):
+            for h in range(2):
+                zt, _src, copy = own_tile(j, cc, h)
+
+                @pl.when(jnp.logical_not((zt == z) & (c == cc)))
+                def _():
+                    copy.wait_send()
+
+        @pl.loop(0, 4)
+        def _(zz):
+            fwd_x(j, zz).wait_send()
+
+        @pl.loop(0, 8)
+        def _(s):
+            fwd_core(j, s).wait_send()
+
+
+def fused_shards(
+    hidden_in,
+    w_convb,
+    w_convc,
+    w_convx,
+    w_query,
+    w_key,
+    w_value,
+    conv_taps,
+    gate_cache,
+    w_out_conv,
+    w_out_attn,
+):
+    tok_rows, model = hidden_in.shape
+    total_rows = gate_cache.shape[0]
+    out_rows = tok_rows // 4
+    small = jnp.concatenate(
+        [
+            gate_cache.T,
+            jnp.pad(conv_taps, ((0, 1), (0, total_rows - conv_taps.shape[1]))),
+        ],
+        axis=0,
+    )
+    bf16 = jnp.bfloat16
+    dma = pltpu.SemaphoreType.DMA
+    any_spec = pl.BlockSpec(memory_space=pl.ANY)
+    return pl.pallas_call(
+        fused_kernel,
+        out_shape=jax.ShapeDtypeStruct((out_rows, model), bf16),
+        in_specs=[any_spec] * 10,
+        out_specs=pl.BlockSpec(memory_space=pltpu.VMEM),
+        scratch_shapes=[
+            pltpu.VMEM((2, tok_rows, model), bf16),
+            pltpu.VMEM((3, model, 256), bf16),
+            pltpu.VMEM((8, total_rows), jnp.float32),
+            pltpu.VMEM((3, 2, tok_rows, 256), bf16),
+            pltpu.VMEM(w_out_attn.shape, bf16),
+            pltpu.VMEM(w_out_conv.shape, bf16),
+            pltpu.VMEM((2, 2, tok_rows, 128), bf16),
+            pltpu.VMEM((2, tok_rows, 256), bf16),
+            pltpu.VMEM((2, 2, out_rows, model), bf16),
+            pltpu.VMEM((2, out_rows, model), bf16),
+            pltpu.VMEM((out_rows, model), bf16),
+            pltpu.VMEM((out_rows, model), bf16),
+            dma,
+            dma,
+            dma((3, 2, 2)),
+            dma((3, 8, 2)),
+            dma((3, 4)),
+            dma((3, 8)),
+            dma,
+            dma((2, 3)),
+            dma((2,)),
+            dma((2, 2)),
+            dma((2, 2)),
+            dma((2, 2)),
+            dma((N_CHUNKS,)),
+            dma((N_CHUNKS,)),
+            dma((N_CHUNKS,)),
+            dma((N_CHUNKS,)),
+            dma((2,)),
+        ],
+        compiler_params=pltpu.CompilerParams(collective_id=0, has_side_effects=True),
+    )(
+        small,
+        hidden_in,
+        w_query,
+        w_key,
+        w_value,
+        w_convc,
+        w_convx,
+        w_convb,
+        w_out_attn,
+        w_out_conv,
+    )
+
+
 def solution(mesh):
+    one_device = shards
+    if mesh.shape["sp"] // 4 == 2 and mesh.shape["tp"] == 4:
+        one_device = fused_shards
     return jax.shard_map(
-        shards,
+        one_device,
         mesh=mesh,
         in_specs=(
             P("sp", None),

time: 298 us -> 87.9 us (0.29)
  the two profiles are of different devices: /device:TPU:0 before, /device:TPU:2 now
where the time goes in v1:
time: 87.9 us; the launch traced here: 87.7 us
  Pallas kernels  84.6 us (96%)
  local copies, waits for them, and re-layouts  1.67 us (2%)
  other arithmetic  1.41 us (2%)
    pallas_call x1, Pallas kernels, fused_shards(): pl.pallas_call(fused_kernel, out_shape=jax.ShapeDtypeStruct((out_rows, mo...  84.6 us

profile of v1, /device:TPU:2, one launch (start us, length us, event | category | flops | bytes accessed | tf_op | source)
XLA Modules:
  0.0 87.7 jit_solution(3235841699043072814)
XLA Ops:
  0.0 1.4 %select_maximum_fusion.small_ref = f32[8,2048]{1,0:T(8,128)} fusion(f32[3,256]{1,0:T(4,128)} %param.18, f32[4,2048]{1,0:T(4,128)} %bitcast.1), kind=kLoop, calls=%fused_computation | loop fusion | flops 49152 | bytes 101376 | tf_op jit(solution)/shard_map/concatenate | solution.py:638
  1.4 84.6 %shard_map.109 = bf16[64,2048]{1,0:T(8,128)(2,1)} custom-call(f32[8,2048]{1,0:T(8,128)} %select_maximum_fusion.small_ref, bf16[256,2048]{1,0:T(8,128)(2,1)} %hidden_ref.1, bf16[256,256]{1,0:T(8,128)(2,1)} %wq_ref.1, bf16[256,256]{1,0:T(8,128)(2,1)} %wk_ref.1, bf16[256,256]{1,0:T(8,128)(2,1)} %wv_ref.1, bf16[256,256]{1,0:T(8,128)(2,1)} %wc_ref.1, ...), custom_call_target="tpu_custom_call" | custom-call | tf_op jit(solution)/shard_map/pallas_call | solution.py:648
  86.0 1.7 %copy.13 = bf16[64,2048]{1,0:T(8,128)(2,1)} copy(bf16[64,2048]{1,0:T(8,128)(2,1)} %shard_map.109) | data formatting | bytes 524288

commit v2 on v1

--- a/solution.py
+++ b/solution.py
@@ -164,10 +164,15 @@
 
 MESH = pl.DeviceIdType.MESH
 N_CHUNKS = 4
+N_PIECES = 4
+HID_LAG = 3
+TILES_1 = 1
+TILES_2 = 4
 
 
 def fused_kernel(
-    small_ref,
+    gate_ref,
+    taps_ref,
     hidden_ref,
     wq_ref,
     wk_ref,
@@ -180,7 +185,8 @@
     out_ref,
     hbuf,
     wbuf,
-    small,
+    gate_in,
+    taps_in,
     proj,
     woa,
     woc,
@@ -197,9 +203,11 @@
     s_wx,
     s_wc,
     s_hx,
-    s_hz,
+    s_up,
+    s_down,
     s_hy,
     r_h,
+    r_hy,
     s_act,
     r_act,
     s_core,
@@ -239,49 +247,77 @@
             )
 
     pl.semaphore_signal(barrier, inc=1, device_id=y_mate, device_id_type=MESH)
-    pl.semaphore_wait(barrier, 17)
+    with jax.named_scope("bar"):
+        pl.semaphore_wait(barrier, 17)
 
     root_z = (2 * c + x, (2 * c + x + 1) % 4)
     root_x = (1, 0)
     block_of = (root_z[0] * 2 + 1, root_z[1] * 2)
     seq_mine = ((sp + 7) % 8) // 2
     x_mine, c_mine = seq_mine % 2, seq_mine // 2
+    piece_rows = half_rows // N_PIECES
+
+    def piece(yy, p):
+        return pl.ds(pl.multiple_of(yy * half_rows + p * piece_rows, piece_rows), piece_rows)
+
+    other_rows = pl.ds(pl.multiple_of((1 - y) * half_rows, half_rows), half_rows)
     my_rows = pl.ds(pl.multiple_of(y * half_rows, half_rows), half_rows)
-    other_rows = pl.ds(pl.multiple_of((1 - y) * half_rows, half_rows), half_rows)
-
-    def fan_out(i, src, go):
-        for step in range(1, 4):
-            zz = (z + step) % 4
-            copy = remote(src, hbuf.at[i, my_rows], s_hz.at[i, step - 1], r_h.at[i, 0], at(zz, x, y, c))
-            go(copy)
-
-    def start(copy):
-        copy.start()
-
-    for i in range(2):
-        is_root = z == root_z[i]
-
-        @pl.when(is_root & (x == root_x[i]))
-        def _():
-            fan_out(i, hidden_ref.at[my_rows], start)
-            pltpu.make_async_copy(
-                hidden_ref.at[my_rows], hbuf.at[i, my_rows], r_h.at[i, 0]
-            ).start()
-            pltpu.make_async_copy(
-                hidden_ref.at[other_rows], hbuf.at[i, other_rows], r_h.at[i, 1]
-            ).start()
-
-    def inject_copy():
+
+    def has_local(i):
+        return (z == root_z[i]) & (x == root_x[i])
+
+    def hid_up(i, p, src):
+        return remote(
+            src, hbuf.at[i, piece(y, p)], s_up.at[i, p], r_h.at[i, p], at(z + 1, x, y, c)
+        )
+
+    def hid_down(i, p, src):
+        return remote(
+            src, hbuf.at[i, piece(y, p)], s_down.at[i, p], r_h.at[i, p], at(z - 1, x, y, c)
+        )
+
+    def hid_y(i, p):
+        part = hbuf.at[i, piece(y, p)]
+        return remote(part, part, s_hy.at[i, p], r_hy.at[i, p], y_mate)
+
+    def goes_up(i):
+        return (z >= root_z[i]) & (z < 3)
+
+    def goes_down(i):
+        return (z <= root_z[i]) & (z > 0)
+
+    def inject_copy(p):
         slot = 1 - x
         return remote(
-            hidden_ref.at[my_rows], hbuf.at[slot, my_rows], s_hx, r_h.at[slot, 0], x_mate
+            hidden_ref.at[piece(y, p)],
+            hbuf.at[slot, piece(y, p)],
+            s_hx.at[p],
+            r_h.at[slot, p],
+            x_mate,
         )
 
     injects = (c == c_mine) & (x_mine != x)
 
     @pl.when(injects)
     def _():
-        inject_copy().start()
+        for p in range(N_PIECES):
+            inject_copy(p).start()
+
+    for i in range(2):
+
+        @pl.when(has_local(i) & goes_up(i))
+        def _():
+            for p in range(N_PIECES):
+                hid_up(i, p, hidden_ref.at[piece(y, p)]).start()
+
+        @pl.when(has_local(i) & goes_down(i))
+        def _():
+            for p in range(N_PIECES):
+                hid_down(i, p, hidden_ref.at[piece(y, p)]).start()
+
+        @pl.when(has_local(i))
+        def _():
+            pltpu.make_async_copy(hidden_ref, hbuf.at[i], r_h.at[i, 0]).start()
 
     sources = (wq_ref, wk_ref, wv_ref, wc_ref, wx_ref, wb_ref)
 
@@ -299,7 +335,7 @@
             src, tile(j, sp, cc), s_w.at[j, cc, h], r_w.at[j, sp, cc], at(zt, x, y, cc)
         )
 
-    for j in range(3):
+    def start_tiles(j):
         for cc in range(2):
             for h in range(2):
                 zt, src, copy = own_tile(j, cc, h)
@@ -313,12 +349,19 @@
                 def _():
                     copy.start()
 
-    small_copy = remote(small_ref, small, s_small, r_small, core_mate)
+    start_tiles(0)
+
+    small_copies = (
+        remote(gate_ref, gate_in, s_small.at[0], r_small.at[0], core_mate),
+        remote(taps_ref, taps_in, s_small.at[1], r_small.at[1], core_mate),
+    )
 
     @pl.when(c == owner_core)
     def _():
-        small_copy.start()
-        pltpu.make_async_copy(small_ref, small, r_small).start()
+        for copy in small_copies:
+            copy.start()
+        pltpu.make_async_copy(gate_ref, gate_in, r_small.at[0]).start()
+        pltpu.make_async_copy(taps_ref, taps_in, r_small.at[1]).start()
 
     wo_copies = (
         pltpu.make_async_copy(woa_ref, woa, l_wo.at[0]),
@@ -327,24 +370,32 @@
     for copy in wo_copies:
         copy.start()
 
-    def hid_y(i):
-        return remote(
-            hbuf.at[i, my_rows], hbuf.at[i, my_rows], s_hy.at[i], r_h.at[i, 1], y_mate
-        )
-
-    def hid_wait(i, k, part):
-        remote(hbuf.at[i, part], hbuf.at[i, part], s_hy.at[i], r_h.at[i, k], y_mate).wait_recv()
-
-    def has_local(i):
-        return (z == root_z[i]) & (x == root_x[i])
-
-    for i in range(2):
-
-        @pl.when((z == root_z[i]) & (x != root_x[i]))
+    def hid_pass(i, p):
+        @pl.when(jnp.logical_not(has_local(i)))
         def _():
-            hid_wait(i, 0, my_rows)
-            fan_out(i, hbuf.at[i, my_rows], start)
-            hid_y(i).start()
+            part = hbuf.at[i, piece(y, p)]
+            remote(part, part, s_hy.at[i, p], r_h.at[i, p], y_mate).wait_recv()
+
+            @pl.when(goes_up(i))
+            def _():
+                hid_up(i, p, part).start()
+
+            @pl.when(goes_down(i))
+            def _():
+                hid_down(i, p, part).start()
+
+            hid_y(i, p).start()
+
+    def hid_rest(i):
+        @pl.when(has_local(i))
+        def _():
+            pltpu.make_async_copy(hidden_ref, hbuf.at[i], r_h.at[i, 0]).wait()
+
+        @pl.when(jnp.logical_not(has_local(i)))
+        def _():
+            for p in range(N_PIECES):
+                part = hbuf.at[i, piece(1 - y, p)]
+                remote(part, part, s_hy.at[i, p], r_hy.at[i, p], y_mate).wait_recv()
 
     def fwd_x(j, zz):
         t = tile(j, zz * 2 + x, c)
@@ -358,20 +409,18 @@
         t = tile(j, s, cc)
         remote(t, t, s_wc.at[j, s], r_w.at[j, s, cc], core_mate).wait_recv()
 
-    def line_forward(j):
-        @pl.loop(0, 4)
-        def _(k):
-            zz = (z + k) % 4
-            tile_wait(j, zz * 2 + x, c)
-            fwd_x(j, zz).start()
-            fwd_core(j, zz * 2 + x).start()
-
-    def cross_forward(j):
-        @pl.loop(0, 4)
-        def _(k):
-            zz = (z + k) % 4
-            tile_wait(j, zz * 2 + 1 - x, c)
-            fwd_core(j, zz * 2 + 1 - x).start()
+    z_near = (z, (z // 2) * 2 + 1 - z % 2, 2 - z // 2, 3 * (1 - z // 2))
+
+    def line_forward(t):
+        j, zz = t // 4, z_near[t % 4]
+        tile_wait(j, zz * 2 + x, c)
+        fwd_x(j, zz).start()
+        fwd_core(j, zz * 2 + x).start()
+
+    def cross_forward(t):
+        j, zz = t // 4, z_near[t % 4]
+        tile_wait(j, zz * 2 + 1 - x, c)
+        fwd_core(j, zz * 2 + 1 - x).start()
 
     def mate_wait(j):
         @pl.loop(0, 8)
@@ -385,43 +434,31 @@
                 hbuf[i], wbuf[j], preferred_element_type=jnp.float32
             ).astype(jnp.bfloat16)
 
-    line_forward(0)
-    for i in range(2):
-
-        @pl.when(z != root_z[i])
-        def _():
-            hid_wait(i, 0, my_rows)
-            hid_y(i).start()
-
-        @pl.when(has_local(i))
-        def _():
-            hid_wait(i, 0, my_rows)
-
-    cross_forward(0)
-    line_forward(1)
-    cross_forward(1)
-    for i in range(2):
-        hid_wait(i, 1, other_rows)
-    mate_wait(0)
-    project_pair(0)
-    mate_wait(1)
-    project_pair(1)
-    line_forward(2)
-    cross_forward(2)
-
-    pltpu.make_async_copy(small_ref, small, r_small).wait()
+    dist = [jnp.abs(z - root_z[i]) for i in range(2)]
+    near_0 = dist[0] <= dist[1]
+
+    def hid_turn(near, p):
+        for i in range(2):
+
+            @pl.when(near_0 if (i == 0) == near else jnp.logical_not(near_0))
+            def _():
+                hid_pass(i, p)
+
+    pltpu.make_async_copy(gate_ref, gate_in, r_small.at[0]).wait()
+    pltpu.make_async_copy(taps_ref, taps_in, r_small.at[1]).wait()
 
     depth = 64
     lane_head = lax.broadcasted_iota(jnp.int32, (rows, 128), 1) // depth
     gates = [
-        small[:, pl.ds(pl.multiple_of(block_of[i] * rows, rows), rows)] for i in range(2)
+        gate_in[:, pl.ds(pl.multiple_of(block_of[i] * rows, rows), rows)] for i in range(2)
     ]
-    gates_t = [g.T for g in gates]
+    gates_t = [jnp.concatenate([g, g], axis=0).T for g in gates]
     causal = lax.broadcasted_iota(jnp.int32, (rows, rows), 0) >= lax.broadcasted_iota(
         jnp.int32, (rows, rows), 1
     )
     first = half_h == 0
-    for i in range(2):
+
+    def attend(i):
         q = proj[0, i, :, :128]
         merged = None
         for hh in range(2):
@@ -495,9 +532,42 @@
                 core_mate,
             ).wait_recv()
 
-    send_acts(0)
-
-    mate_wait(2)
+    for t in range(12):
+        with jax.named_scope(f"h{t}"):
+            if t < N_PIECES:
+                hid_turn(True, t)
+            if HID_LAG <= t < HID_LAG + N_PIECES:
+                hid_turn(False, t - HID_LAG)
+        if t == TILES_1:
+            start_tiles(1)
+        if t == TILES_2:
+            start_tiles(2)
+        with jax.named_scope(f"l{t}"):
+            line_forward(t)
+            if t >= 1:
+                cross_forward(t - 1)
+        if t == 7:
+            with jax.named_scope("hrest"):
+                for i in range(2):
+                    hid_rest(i)
+            with jax.named_scope("mw0"):
+                mate_wait(0)
+            project_pair(0)
+        if t == 8:
+            with jax.named_scope("mw1"):
+                mate_wait(1)
+            project_pair(1)
+        if t == 9:
+            attend(0)
+        if t == 10:
+            attend(1)
+            with jax.named_scope("sa0"):
+                send_acts(0)
+    cross_forward(11)
+
+
+    with jax.named_scope("mw2"):
+        mate_wait(2)
     project_pair(2)
     row_id = lax.broadcasted_iota(jnp.int32, (2 * rows, 128), 0)
     gate_c = jnp.concatenate([proj[1, 0, :, 128:], proj[1, 1, :, 128:]], axis=0)
@@ -508,7 +578,7 @@
         .astype(jnp.bfloat16)
         .astype(jnp.float32)
     )
-    taps = [jnp.where(first, small[4 + k : 5 + k, :128], small[4 + k : 5 + k, 128:256]) for k in range(3)]
+    taps = [jnp.where(first, taps_in[k : k + 1, :128], taps_in[k : k + 1, 128:]) for k in range(3)]
     mixed = taps[2] * conv_in
     for back in (1, 2):
         moved = jnp.where(row_id >= back, pltpu.roll(conv_in, back, 0), 0.0)
@@ -516,12 +586,15 @@
     conv_out = (gate_b.astype(jnp.float32) * mixed).astype(jnp.bfloat16)
     acts[1, 0] = conv_out[:rows]
     acts[1, 1] = conv_out[rows:]
-    send_acts(1)
+    with jax.named_scope("sa1"):
+        send_acts(1)
 
     for copy in wo_copies:
         copy.wait()
-    wait_acts(0)
-    wait_acts(1)
+    with jax.named_scope("wa0"):
+        wait_acts(0)
+    with jax.named_scope("wa1"):
+        wait_acts(1)
 
     part_rows = pbuf.shape[2]
     width = pbuf.shape[3] // N_CHUNKS
@@ -560,10 +633,11 @@
         ).astype(jnp.bfloat16)
         y_copy(n).start()
 
-    for n in range(N_CHUNKS):
-        out_chunk(n)
-        if n >= 1:
-            pass_chunk(n - 1)
+    with jax.named_scope("outc"):
+        for n in range(N_CHUNKS):
+            out_chunk(n)
+            if n >= 1:
+                pass_chunk(n - 1)
     pass_chunk(N_CHUNKS - 1)
     for n in range(N_CHUNKS):
         y_copy(n).wait_recv()
@@ -585,21 +659,29 @@
 
     @pl.when(c == owner_core)
     def _():
-        small_copy.wait_send()
+        for copy in small_copies:
+            copy.wait_send()
 
     @pl.when(injects)
     def _():
-        inject_copy().wait_send()
+        for p in range(N_PIECES):
+            inject_copy(p).wait_send()
 
     for i in range(2):
-
-        @pl.when(z == root_z[i])
-        def _():
-            fan_out(i, hbuf.at[i, my_rows], lambda copy: copy.wait_send())
-
-        @pl.when(jnp.logical_not(has_local(i)))
-        def _():
-            hid_y(i).wait_send()
+        for p in range(N_PIECES):
+            part = hbuf.at[i, piece(y, p)]
+
+            @pl.when(goes_up(i))
+            def _():
+                hid_up(i, p, part).wait_send()
+
+            @pl.when(goes_down(i))
+            def _():
+                hid_down(i, p, part).wait_send()
+
+            @pl.when(jnp.logical_not(has_local(i)))
+            def _():
+                hid_y(i, p).wait_send()
 
     for j in range(3):
         for cc in range(2):
@@ -635,25 +717,19 @@
     tok_rows, model = hidden_in.shape
     total_rows = gate_cache.shape[0]
     out_rows = tok_rows // 4
-    small = jnp.concatenate(
-        [
-            gate_cache.T,
-            jnp.pad(conv_taps, ((0, 1), (0, total_rows - conv_taps.shape[1]))),
-        ],
-        axis=0,
-    )
     bf16 = jnp.bfloat16
     dma = pltpu.SemaphoreType.DMA
     any_spec = pl.BlockSpec(memory_space=pl.ANY)
     return pl.pallas_call(
         fused_kernel,
         out_shape=jax.ShapeDtypeStruct((out_rows, model), bf16),
-        in_specs=[any_spec] * 10,
+        in_specs=[any_spec] * 11,
         out_specs=pl.BlockSpec(memory_space=pltpu.VMEM),
         scratch_shapes=[
             pltpu.VMEM((2, tok_rows, model), bf16),
             pltpu.VMEM((3, model, 256), bf16),
-            pltpu.VMEM((8, total_rows), jnp.float32),
+            pltpu.VMEM((gate_cache.shape[1], total_rows), jnp.float32),
+            pltpu.VMEM(conv_taps.shape, jnp.float32),
             pltpu.VMEM((3, 2, tok_rows, 256), bf16),
             pltpu.VMEM(w_out_attn.shape, bf16),
             pltpu.VMEM(w_out_conv.shape, bf16),
@@ -663,16 +739,18 @@
             pltpu.VMEM((2, out_rows, model), bf16),
             pltpu.VMEM((out_rows, model), bf16),
             pltpu.VMEM((out_rows, model), bf16),
-            dma,
-            dma,
+            dma((2,)),
+            dma((2,)),
             dma((3, 2, 2)),
             dma((3, 8, 2)),
             dma((3, 4)),
             dma((3, 8)),
-            dma,
-            dma((2, 3)),
-            dma((2,)),
-            dma((2, 2)),
+            dma((N_PIECES,)),
+            dma((2, N_PIECES)),
+            dma((2, N_PIECES)),
+            dma((2, N_PIECES)),
+            dma((2, N_PIECES)),
+            dma((2, N_PIECES)),
             dma((2, 2)),
             dma((2, 2)),
             dma((N_CHUNKS,)),
@@ -683,7 +761,8 @@
         ],
         compiler_params=pltpu.CompilerParams(collective_id=0, has_side_effects=True),
     )(
-        small,
+        gate_cache.T,
+        conv_taps,
         hidden_in,
         w_query,
         w_key,

time: 87.9 us -> 75.8 us (0.86)
  the two profiles are of different devices: /device:TPU:2 before, /device:TPU:0 now
where the time goes in v2:
time: 75.8 us; the launch traced here: 75.7 us
  Pallas kernels  74 us (98%)
  local copies, waits for them, and re-layouts  1.67 us (2%)
    pallas_call x1, Pallas kernels, fused_shards(): pl.pallas_call(fused_kernel, out_shape=jax.ShapeDtypeStruct((out_rows, mo...  74 us
    unnamed x1, local copies, waits for them, and re-layouts  1.67 us

profile of v2, /device:TPU:0, one launch (start us, length us, event | category | flops | bytes accessed | tf_op | source)
XLA Modules:
  0.0 75.7 jit_solution(15710985081215281930)
XLA Ops:
  0.0 74.0 %shard_map.109 = bf16[64,2048]{1,0:T(8,128)(2,1)} custom-call(f32[4,2048]{1,0:T(4,128)} %bitcast.1, f32[3,256]{1,0:T(4,128)} %taps_ref.1, bf16[256,2048]{1,0:T(8,128)(2,1)} %hidden_ref.1, bf16[256,256]{1,0:T(8,128)(2,1)} %wq_ref.1, bf16[256,256]{1,0:T(8,128)(2,1)} %wk_ref.1, bf16[256,256]{1,0:T(8,128)(2,1)} %wv_ref.1, bf16[256,256]{1,0:T(8,128)(2,1)} %wc_ref.1, ...), custom_call_target="tpu_custom_call" | custom-call | tf_op jit(solution)/shard_map/pallas_call | solution.py:723
  74.0 1.7 %copy.13 = bf16[64,2048]{1,0:T(8,128)(2,1)} copy(bf16[64,2048]{1,0:T(8,128)(2,1)} %shard_map.109) | data formatting | bytes 524288
